TPU v7x, 512 devices: a whole 4x8x8 slice. The times are simulated.
512 devices in a mesh: sp: 32 (over z, x), tp: 16 (over y, core).
Axes of the slice: x: 4, y: 8, z: 8, core: 2. Of those that a mesh axis runs over, the one named last changes fastest.
Arguments:
- mixed: bfloat16 [4096, 2048], P('sp'), may hold values from -6 to 6
- cotangent: bfloat16 [4096, 2048], P('sp'), may hold values from -6 to 6
- routes: int32 [4096, 2], P('sp'), may hold values from 0 to 31, all different within a row; in each aligned block of 128 rows (0 to 127, 128 to 255, ...) at most 16 rows name the same one
- gates: float32 [4096, 2], P('sp'), may hold values from 0.1 to 1
- w_gate: bfloat16 [32, 2048, 1024], P('sp', None, 'tp'), may hold values from -0.125 to 0.125
- w_up: bfloat16 [32, 2048, 1024], P('sp', None, 'tp'), may hold values from -0.125 to 0.125
- w_down: bfloat16 [32, 1024, 2048], P('sp', 'tp'), may hold values from -0.1875 to 0.1875
- out_weight: bfloat16 [4096, 2048], P('tp'), may hold values from -0.09375 to 0.09375
- gate_pre: bfloat16 [4096, 4096], P('sp', 'tp'), may hold values from -8 to 8
- mixer_out: bfloat16 [4096, 4096], P('sp', 'tp'), may hold values from -6 to 6
- values: bfloat16 [4096, 4096], P('sp', 'tp'), may hold values from -6 to 6
- write_keys: bfloat16 [4096, 2048], P('sp', 'tp'), may hold values from -1.25 to 1.25
- read_keys: bfloat16 [4096, 2048], P('sp', 'tp'), may hold values from -1.25 to 1.25
- log_decay: float32 [64, 4096], P('tp', 'sp'), may hold values from -0.08 to 0
- entry_states: float32 [32, 64, 64, 128], P('sp', 'tp'), may hold values from -6 to 6
Outputs:
- d_w_gate: bfloat16 [32, 2048, 1024], P('sp', None, 'tp')
- d_w_up: bfloat16 [32, 2048, 1024], P('sp', None, 'tp')
- d_w_down: bfloat16 [32, 1024, 2048], P('sp', 'tp')
- d_out_weight: float32 [2048, 4096], P('sp', 'tp')
- d_input: bfloat16 [4096, 2048], P('sp', 'tp')
- d_values: bfloat16 [4096, 4096], P('sp', 'tp')
- d_write: float32 [4096, 2048], P('sp', 'tp')
- d_read: float32 [4096, 2048], P('sp', 'tp')
- d_gate: bfloat16 [4096, 4096], P('sp', 'tp')
Inputs may be any that keep to these rules, and one draw needn't show every extreme that they name: `routes`: each row names 2 different experts; in the 128 rows of one device no expert is named more than 16 times, and in some blocks one is named exactly 16 times.
All inputs are finite; a program needn't handle non-finite values.
Results may differ from a plain program's by a relative error of at most 0.0062.
Values may be sent and summed in bfloat16 or wider, within the bound.
No kernel may reach another device: no remote copies, remote signals or barrier semaphores. Data moves between devices by JAX's collectives and lax.ppermute only.
A program may use at most 64 MiB of HBM per device.

v0:
```python
import jax
import jax.numpy as jnp
from jax import lax
from jax.sharding import Mesh
from jax.sharding import PartitionSpec as P

D = 2048
HEAD_DIM = 64
BLOCK = 128
TOPK = 2
TOK_DEV = 128
SP = ("sp_0", "sp_1")
precise = lax.Precision.HIGHEST


def sent_together(arrays, axis, split_dim, concat_dim, along):
    widths = [a.shape[along] for a in arrays]
    both = jnp.concatenate(arrays, axis=along)
    out = lax.all_to_all(both, axis, split_axis=split_dim, concat_axis=concat_dim, tiled=True)
    return tuple(jnp.split(out, [sum(widths[:k]) for k in range(1, len(widths))], axis=along))


def in_one_piece(arrays, axis, dim, along):
    widths = [a.shape[along] for a in arrays]
    both = jnp.concatenate(arrays, axis=along)
    out = lax.all_gather(both, axis, axis=dim, tiled=True)
    return tuple(jnp.split(out, [sum(widths[:k]) for k in range(1, len(widths))], axis=along))


def split_up(value, dim, count):
    before, after = (value.shape[:dim], value.shape[dim + 1 :])
    return jnp.moveaxis(value.reshape(*before, count, -1, *after), dim, 0)


def sent_and_summed(value, axis, dim):
    count = lax.axis_size(axis)
    parts = lax.all_to_all(split_up(value, dim, count), axis, 0, 0, tiled=True)
    return jnp.sum(parts, axis=0)


def filled_with(value, identity):
    return jax.tree.map(
        lambda a, e: jnp.broadcast_to(jnp.asarray(e, a.dtype), a.shape), value, identity
    )


def prefix_by_axis(value, axes, combine, identity):
    before = start = filled_with(value, identity)
    running = value
    for axis in reversed(axes):
        count, mine = (lax.axis_size(axis), lax.axis_index(axis))
        pieces = jax.tree.map(lambda part: lax.all_gather(part, axis), running)
        inside, running = (start, start)
        for k in reversed(range(count)):
            passed = k > mine
            running = combine(running, jax.tree.map(lambda part: part[k], pieces))
            inside = jax.tree.map(lambda new, old: jnp.where(passed, new, old), running, inside)
        before = combine(inside, before)
    return before


def silu_grad(pre_act):
    logistic = jax.nn.sigmoid(pre_act)
    return logistic * (1.0 + pre_act * (1.0 - logistic))


def contract_rows(first_op, second_op):
    return lax.dot_general(
        first_op, second_op, (((0,), (0,)), ((), ())), preferred_element_type=jnp.float32
    )


def contract_cols(first_op, second_op):
    return lax.dot_general(
        first_op, second_op, (((1,), (1,)), ((), ())), preferred_element_type=jnp.float32
    )


def combine_state(earlier, later):
    return (later[0] * earlier[0], later[1] + later[0][:, None, None] * earlier[1])


def block_back(grad_state, inputs_x, grad_y, log_rate, write_rows, read_rows, start_state):
    block_len = log_rate.shape[0]
    running = jnp.cumsum(log_rate, axis=0)
    causal_mask = (jnp.arange(block_len)[:, None] >= jnp.arange(block_len)[None, :])[:, :, None]
    spread = running[:, None, :] - running[None, :, :]
    decay_mat = jnp.where(causal_mask, jnp.exp(jnp.where(causal_mask, spread, 0.0)), 0.0)
    intersection = jnp.dot(read_rows, write_rows.T, precision=precise)
    mixing = intersection[:, :, None] * decay_mat
    to_end = jnp.exp(running[-1][None, :] - running)
    from_start = jnp.exp(running)
    grad_x = jnp.einsum("lsj,ljp->sjp", mixing, grad_y, precision=precise) + to_end[
        :, :, None
    ] * jnp.einsum("sn,jpn->sjp", write_rows, grad_state, precision=precise)
    weighted = jnp.einsum("ljp,sjp->lsj", grad_y, inputs_x, precision=precise) * decay_mat
    grad_w = jnp.einsum("lsj,ln->sn", weighted, read_rows, precision=precise) + jnp.einsum(
        "sj,sjp,jpn->sn", to_end, inputs_x, grad_state, precision=precise
    )
    grad_r = jnp.einsum("lsj,sn->ln", weighted, write_rows, precision=precise) + jnp.einsum(
        "lj,ljp,jpn->ln", from_start, grad_y, start_state, precision=precise
    )
    earlier = jnp.exp(running[-1])[:, None, None] * grad_state + jnp.einsum(
        "lj,ljp,ln->jpn", from_start, grad_y, read_rows, precision=precise
    )
    return (earlier, grad_x, grad_w, grad_r)


def body(
    mixed,
    cotangent,
    routes,
    gates,
    w_gate,
    w_up,
    w_down,
    out_weight,
    gate_pre,
    mixer_out,
    values,
    write_keys,
    read_keys,
    log_decay,
    entry_states,
):
    sp_count = lax.axis_size(SP)
    tp_count = lax.axis_size("tp")
    capacity = 4 * TOK_DEV // sp_count
    assigned = TOK_DEV * TOPK
    picks = routes.reshape(assigned)
    onehot = (picks[:, None] == jnp.arange(sp_count, dtype=jnp.int32)[None, :]).astype(jnp.int32)
    earlier_same = jnp.cumsum(onehot, axis=0) - onehot
    slot_of = jnp.sum(earlier_same * onehot, axis=1)
    target = picks * capacity + slot_of
    anchor = (
        jnp.full((sp_count * capacity,), assigned, jnp.int32)
        .at[target]
        .set(jnp.arange(assigned, dtype=jnp.int32))
    )
    weight_g = w_gate[0]
    weight_u = w_up[0]
    weight_d = w_down[0]
    column_count = D // tp_count
    offset = lax.axis_index("tp") * column_count
    tok_slice = lax.dynamic_slice_in_dim(mixed, offset, column_count, 1)
    cot_slice = lax.dynamic_slice_in_dim(cotangent, offset, column_count, 1)
    columns = tok_slice.shape[1]
    scaled = (
        (gates[:, :, None] * cot_slice[:, None, :].astype(jnp.float32))
        .astype(jnp.bfloat16)
        .reshape(assigned, columns)
    )
    empty_row = jnp.zeros((1, columns), jnp.bfloat16)
    cot_buffer = jnp.concatenate([scaled, empty_row])[anchor].reshape(sp_count, capacity, columns)
    tok_buffer = jnp.concatenate([tok_slice, empty_row])[anchor // TOPK].reshape(
        sp_count, capacity, columns
    )
    tok_buffer, cot_buffer = (tok_buffer, cot_buffer)
    tok_part, cot_part = sent_together((tok_buffer, cot_buffer), SP, 0, 0, 1)
    tok_rows, cot_rows = in_one_piece((tok_part, cot_part), "tp", 2, 0)
    expert_tok_rows = tok_rows
    expert_cot_rows = cot_rows
    expert_tok_rows = expert_tok_rows.reshape(-1, D)
    expert_cot_rows = expert_cot_rows.reshape(-1, D)
    pre_gate = jnp.dot(expert_tok_rows, weight_g, preferred_element_type=jnp.float32)
    pre_up = jnp.dot(expert_tok_rows, weight_u, preferred_element_type=jnp.float32)
    active = jax.nn.silu(pre_gate)
    hidden = (active * pre_up).astype(jnp.bfloat16)
    grad_down = contract_rows(hidden, expert_cot_rows)
    grad_hidden = contract_cols(expert_cot_rows, weight_d)
    grad_gate = (grad_hidden * pre_up * silu_grad(pre_gate)).astype(jnp.bfloat16)
    grad_upval = (grad_hidden * active).astype(jnp.bfloat16)
    grad_wg = contract_rows(expert_tok_rows, grad_gate)
    grad_wu = contract_rows(expert_tok_rows, grad_upval)
    partial_value = contract_cols(grad_gate, weight_g) + contract_cols(grad_upval, weight_u)
    grad_wg, grad_wu, grad_down, partial_value = (grad_wg, grad_wu, grad_down, partial_value)
    row_total = partial_value.shape[0]
    pieces = partial_value.astype(jnp.bfloat16).reshape(row_total, tp_count, column_count)
    received = lax.all_to_all(pieces, "tp", split_axis=1, concat_axis=1, tiled=True)
    summed = (
        jnp.sum(received.astype(jnp.float32), axis=1)
        .astype(jnp.bfloat16)
        .reshape(sp_count, capacity, column_count)
    )
    returned = lax.all_to_all(summed, SP, split_axis=0, concat_axis=0, tiled=True)
    columns = returned.shape[-1]
    picked = returned.reshape(sp_count * capacity, columns)[target].reshape(TOK_DEV, TOPK, columns)
    d_input = (cot_slice.astype(jnp.float32) + jnp.sum(picked.astype(jnp.float32), axis=1)).astype(
        jnp.bfloat16
    )
    whole = lax.all_gather(d_input, "tp", axis=1, tiled=True)
    back_proj = contract_cols(whole, out_weight)
    pre_act = gate_pre.astype(jnp.float32)
    gate_act = jax.nn.silu(pre_act)
    saved_out = mixer_out.astype(jnp.float32)
    d_gate = (back_proj * saved_out * silu_grad(pre_act)).astype(jnp.bfloat16)
    gated = (saved_out * gate_act).astype(jnp.bfloat16)
    d_out_weight = sent_and_summed(contract_rows(whole, gated), SP, 0)
    head_count = out_weight.shape[0] // HEAD_DIM
    grad_y = (back_proj * gate_act).reshape(TOK_DEV, head_count, HEAD_DIM)
    inputs_x = values.astype(jnp.float32).reshape(TOK_DEV, head_count, HEAD_DIM)
    write_rows = write_keys.astype(jnp.float32)
    read_rows = read_keys.astype(jnp.float32)
    log_rate = log_decay.T
    total_run = jnp.cumsum(log_rate, axis=0)
    shard_decay = jnp.exp(total_run[-1])
    shard_grad = jnp.einsum(
        "lj,ljp,ln->jpn", jnp.exp(total_run), grad_y, read_rows, precision=precise
    )
    identity = (jnp.ones_like(shard_decay), jnp.zeros_like(shard_grad))
    incoming = prefix_by_axis((shard_decay, shard_grad), SP, combine_state, identity)
    grad_state = incoming[1]
    pieces_x = []
    pieces_w = []
    pieces_r = []
    for block_id in reversed(range(TOK_DEV // BLOCK)):
        grad_state, grad_x, grad_w, grad_r = block_back(
            grad_state, inputs_x, grad_y, log_rate, write_rows, read_rows, entry_states[block_id]
        )
        pieces_x.insert(0, grad_x)
        pieces_w.insert(0, grad_w)
        pieces_r.insert(0, grad_r)
    d_values = pieces_x[0].reshape(TOK_DEV, head_count * HEAD_DIM).astype(jnp.bfloat16)
    d_write = pieces_w[0]
    d_read = pieces_r[0]
    return (
        grad_wg.astype(jnp.bfloat16)[None],
        grad_wu.astype(jnp.bfloat16)[None],
        grad_down.astype(jnp.bfloat16)[None],
        d_out_weight,
        d_input,
        d_values,
        d_write,
        d_read,
        d_gate,
    )


def solution(mesh):
    finer = Mesh(mesh.devices.reshape(8, 4, mesh.shape["tp"]), ("sp_0", "sp_1", "tp"))
    return jax.shard_map(
        body,
        mesh=finer,
        in_specs=(
            P(SP, None),
            P(SP, None),
            P(SP, None),
            P(SP, None),
            P(SP, None, "tp"),
            P(SP, None, "tp"),
            P(SP, "tp", None),
            P("tp", None),
            P(SP, "tp"),
            P(SP, "tp"),
            P(SP, "tp"),
            P(SP, "tp"),
            P(SP, "tp"),
            P("tp", SP),
            P(SP, "tp", None, None),
        ),
        out_specs=(
            P(SP, None, "tp"),
            P(SP, None, "tp"),
            P(SP, "tp", None),
            P(SP, "tp"),
            P(SP, "tp"),
            P(SP, "tp"),
            P(SP, "tp"),
            P(SP, "tp"),
            P(SP, "tp"),
        ),
        check_vma=False,
    )
```

profile of v0, /device:TPU:2, one launch (start us, length us, event | category | flops | bytes accessed | tf_op | source)
XLA Modules:
  0.0 289.5 jit_solution(18188501029784762102)
XLA Ops:
  11.2 1.4 scatter_custom_fusion
  13.6 1.3 gather_fusion.1
  15.0 1.3 gather_fusion
  16.4 24.5 %all_to_all.20 = bf16[32,32,128]{2,1,0:T(8,128)(2,1)S(1)} all-to-all(bf16[32,32,128]{2,1,0:T(8,128)(2,1)S(1)} %pad_maximum_fusion), channel_id=1, replica_groups=mesh['sp_0'=8,'sp_1'=4,'tp'=16] {'sp_0','sp_1'}, dimensions={0} | all-to-all | bytes 524288 | tf_op jit(solution)/shard_map/all_to_all | solution.py:19
  41.6 48.4 %all-gather.6.cloned.1.call-done = bf16[64,16,2048]{2,1,0:T(8,128)(2,1)} async-done(((bf16[64,16,128]{2,1,0:T(8,128)(2,1)}), bf16[64,16,2048]{2,1,0:T(8,128)(2,1)}) %all-gather.6.cloned.1.call-update) | async-done | bytes 4194320 | tf_op jit(solution)/shard_map/all_gather | solution.py:26
  90.1 2.6 fusion.77
  96.9 1.9 copy.65
  98.8 4.6 %all-to-all-start.1 = ((bf16[512,16,128]{2,0,1:T(8,128)(2,1)}), bf16[512,16,128]{2,0,1:T(8,128)(2,1)}, u32[]{:S(2)}, u32[]{:S(2)}) async-start(bf16[512,16,128]{2,0,1:T(8,128)(2,1)} %bitcast.231), calls=%async_computation.1 | async-start | bytes 4194304 | tf_op jit(solution)/shard_map/all_to_all | solution.py:179
  103.7 49.0 %all-to-all-done.1 = bf16[512,16,128]{2,0,1:T(8,128)(2,1)} async-done(((bf16[512,16,128]{2,0,1:T(8,128)(2,1)}), bf16[512,16,128]{2,0,1:T(8,128)(2,1)}, u32[]{:S(2)}, u32[]{:S(2)}) %all-to-all-start.1) | async-done | bytes 2097184 | tf_op jit(solution)/shard_map/all_to_all | solution.py:179
  152.6 2.6 reduce_sum.56
  155.2 10.5 %all-to-all-start.2 = ((bf16[32,16,128]{2,1,0:T(8,128)(2,1)}), bf16[32,16,128]{2,1,0:T(8,128)(2,1)S(1)}, u32[]{:S(2)}, u32[]{:S(2)}) async-start(bf16[32,16,128]{2,1,0:T(8,128)(2,1)} %bitcast.237), calls=%async_computation.2 | async-start | bytes 262144 | tf_op jit(solution)/shard_map/all_to_all | solution.py:185
  165.7 7.8 %all-gather.1 = f32[4,1,4]{2,1,0:T(1,128)S(1)} all-gather(f32[1,1,4]{2,1,0:T(1,128)S(1)} %get-tuple-element.47), channel_id=1, replica_groups=mesh['sp_0'=8,'sp_1'=4,'tp'=16] {'sp_1'}, dimensions={0}, use_global_device_ids=true | all-gather | bytes 80 | tf_op jit(solution)/shard_map/all_gather | solution.py:52
  176.6 16.8 %all_gather.25 = bf16[128,2048]{1,0:T(8,128)(2,1)S(1)} all-gather(bf16[128,128]{1,0:T(8,128)(2,1)S(1)} %add_convert_fusion.1), channel_id=1, replica_groups=mesh['sp_0'=8,'sp_1'=4,'tp'=16] {'tp'}, dimensions={1}, use_global_device_ids=true | all-gather | bytes 557056 | tf_op jit(solution)/shard_map/all_gather | solution.py:191
  194.3 2.7 fusion.56
  196.9 9.3 %all-to-all-start.3 = ((f32[32,64,256]{2,1,0:T(8,128)}), f32[32,64,256]{2,1,0:T(8,128)}, u32[]{:S(2)}, u32[]{:S(2)}) async-start(f32[32,64,256]{2,1,0:T(8,128)} %bitcast.230), calls=%async_computation.3 | async-start | bytes 4194304 | tf_op jit(solution)/shard_map/all_to_all | solution.py:37
  207.5 2.3 fusion.21
  210.9 18.1 %all-gather = f32[16,64,128]{2,1,0:T(8,128)S(1)} all-gather(f32[4,64,128]{2,1,0:T(8,128)S(1)} %fusion.54), channel_id=2, replica_groups=mesh['sp_0'=8,'sp_1'=4,'tp'=16] {'sp_1'}, dimensions={0}, use_global_device_ids=true | all-gather | bytes 655360 | tf_op jit(solution)/shard_map/all_gather | solution.py:52
  229.8 1.3 fusion.44
  232.8 1.6 copy.59
  234.4 31.3 %all-gather.2 = f32[8,1,4]{2,1,0:T(1,128)S(1)} all-gather(f32[1,1,4]{2,1,0:T(1,128)} %get-tuple-element.58), channel_id=1, replica_groups=mesh['sp_0'=8,'sp_1'=4,'tp'=16] {'sp_0'}, dimensions={0}, use_global_device_ids=true | all-gather | bytes 144 | tf_op jit(solution)/shard_map/all_gather | solution.py:52
  267.1 2.2 fusion.1
  273.5 2.4 all-gather.8.cloned.1.call-done
  276.0 1.6 fusion.37
  280.3 2.3 reduce_sum.58
  (147 shorter events, 27.0 us)
Async XLA Ops:
  7.2 200.3 %copy-start = (bf16[256,2048]{1,0:T(8,128)(2,1)S(1)}, bf16[256,2048]{1,0:T(8,128)(2,1)}, u32[]{:S(2)}) copy-start(bf16[256,2048]{1,0:T(8,128)(2,1)} %param.22) | copy-start | bytes 3145732
  7.2 82.9 %all-gather.6.cloned.1.call-start = ((), (), s32[]{:S(2)}) async-start(), calls=%async_computation.4 | async-start | bytes 4456448 | tf_op jit(solution)/shard_map/all_gather | solution.py:26
  41.6 51.1 %copy-start.6 = (bf16[1,2048,64]{1,2,0:T(8,128)(2,1)S(1)}, bf16[1,2048,64]{1,2,0:T(8,128)(2,1)}, u32[]{:S(2)}) copy-start(bf16[1,2048,64]{1,2,0:T(8,128)(2,1)} %param.19) | copy-start | bytes 786436
  98.8 53.9 %all-to-all-start.1 = ((bf16[512,16,128]{2,0,1:T(8,128)(2,1)}), bf16[512,16,128]{2,0,1:T(8,128)(2,1)}, u32[]{:S(2)}, u32[]{:S(2)}) async-start(bf16[512,16,128]{2,0,1:T(8,128)(2,1)} %bitcast.231), calls=%async_computation.1 | async-start | bytes 4194304 | tf_op jit(solution)/shard_map/all_to_all | solution.py:179
  155.2 19.6 %all-to-all-start.2 = ((bf16[32,16,128]{2,1,0:T(8,128)(2,1)}), bf16[32,16,128]{2,1,0:T(8,128)(2,1)S(1)}, u32[]{:S(2)}, u32[]{:S(2)}) async-start(bf16[32,16,128]{2,1,0:T(8,128)(2,1)} %bitcast.237), calls=%async_computation.2 | async-start | bytes 262144 | tf_op jit(solution)/shard_map/all_to_all | solution.py:185
  176.6 20.3 %copy-start.21 = (bf16[128,128]{1,0:T(8,128)(2,1)}, bf16[128,128]{1,0:T(8,128)(2,1)S(1)}, u32[]{:S(2)}) copy-start(bf16[128,128]{1,0:T(8,128)(2,1)S(1)} %add_convert_fusion.1) | copy-start | bytes 98308
  196.9 9.9 %copy-start.17 = (f32[128,4]{1,0:T(8,128)S(1)}, f32[128,4]{1,0:T(8,128)}, u32[]{:S(2)}) copy-start(f32[128,4]{1,0:T(8,128)} %get-tuple-element.45) | copy-start | bytes 6148
  196.9 83.4 %all-to-all-start.3 = ((f32[32,64,256]{2,1,0:T(8,128)}), f32[32,64,256]{2,1,0:T(8,128)}, u32[]{:S(2)}, u32[]{:S(2)}) async-start(f32[32,64,256]{2,1,0:T(8,128)} %bitcast.230), calls=%async_computation.3 | async-start | bytes 4194304 | tf_op jit(solution)/shard_map/all_to_all | solution.py:37
  206.3 69.6 %all-gather.8.cloned.1.call-start = ((), (), s32[]{:S(2)}) async-start(), calls=%async_computation.5 | async-start | bytes 1179648 | tf_op jit(solution)/shard_map/all_gather | solution.py:52
  207.4 22.4 %copy-start.25 = (f32[4]{0:T(128)S(1)}, f32[4]{0:T(128)}, u32[]{:S(2)}) copy-start(f32[4]{0:T(128)} %get-tuple-element.60) | copy-start | bytes 52
  207.5 58.9 %copy-start.10 = (bf16[128,128]{1,0:T(8,128)(2,1)S(1)}, bf16[128,128]{1,0:T(8,128)(2,1)}, u32[]{:S(2)}) copy-start(bf16[128,128]{1,0:T(8,128)(2,1)} %param.26) | copy-start | bytes 98308
  234.4 34.9 %copy-start.15 = (bf16[512,64]{0,1:T(8,128)(2,1)S(1)}, bf16[512,64]{0,1:T(8,128)(2,1)}, u32[]{:S(2)}) copy-start(bf16[512,64]{0,1:T(8,128)(2,1)} %copy-done.14) | copy-start | bytes 196612
  265.7 6.5 %copy-start.23 = (pred[128,128]{1,0:T(8,128)(4,1)}, pred[128,128]{1,0:T(8,128)(4,1)S(1)}, u32[]{:S(2)}) copy-start(pred[128,128]{1,0:T(8,128)(4,1)S(1)} %iota_compare_fusion) | copy-start | bytes 49156
  270.5 5.4 %copy-start.4 = (f32[16,64,128]{2,1,0:T(8,128)S(1)}, f32[16,64,128]{2,1,0:T(8,128)}, u32[]{:S(2)}) copy-start(f32[16,64,128]{2,1,0:T(8,128)} %copy-done.3) | copy-start | bytes 1572868
  270.5 5.4 %copy-start.26 = (f32[4]{0:T(128)S(1)}, f32[4]{0:T(128)}, u32[]{:S(2)}) copy-start(f32[4]{0:T(128)} %get-tuple-element.60) | copy-start | bytes 52
  270.5 5.4 %copy-start.27 = (f32[4]{0:T(128)S(1)}, f32[4]{0:T(128)}, u32[]{:S(2)}) copy-start(f32[4]{0:T(128)} %get-tuple-element.61) | copy-start | bytes 52
  270.5 5.4 %copy-start.28 = (f32[4]{0:T(128)S(1)}, f32[4]{0:T(128)}, u32[]{:S(2)}) copy-start(f32[4]{0:T(128)} %get-tuple-element.56) | copy-start | bytes 52
  270.5 5.4 %copy-start.29 = (f32[4]{0:T(128)S(1)}, f32[4]{0:T(128)}, u32[]{:S(2)}) copy-start(f32[4]{0:T(128)} %get-tuple-element.48) | copy-start | bytes 52
  270.5 5.4 %copy-start.30 = (f32[4]{0:T(128)S(1)}, f32[4]{0:T(128)}, u32[]{:S(2)}) copy-start(f32[4]{0:T(128)} %get-tuple-element.49) | copy-start | bytes 52
  270.5 5.4 %copy-start.31 = (f32[4]{0:T(128)S(1)}, f32[4]{0:T(128)}, u32[]{:S(2)}) copy-start(f32[4]{0:T(128)} %get-tuple-element.50) | copy-start | bytes 52
  271.8 6.0 %copy-start.22 = (f32[128,128]{1,0:T(8,128)S(1)}, f32[128,128]{1,0:T(8,128)}, u32[]{:S(2)}) copy-start(f32[128,128]{1,0:T(8,128)} %fusion.79) | copy-start | bytes 196612
  271.8 6.0 %copy-start.39 = (f32[128,4]{0,1:T(4,128)S(1)}, f32[128,4]{0,1:T(4,128)}, u32[]{:S(2)}) copy-start(f32[128,4]{0,1:T(4,128)} %copy.55) | copy-start | bytes 6148
  271.8 7.3 %copy-start.19 = (bf16[128,256]{0,1:T(8,128)(2,1)S(1)}, bf16[128,256]{0,1:T(8,128)(2,1)}, u32[]{:S(2)}) copy-start(bf16[128,256]{0,1:T(8,128)(2,1)} %copy.59) | copy-start | bytes 196612
  271.8 7.7 %copy-start.13 = (bf16[128,128]{1,0:T(8,128)(2,1)S(1)}, bf16[128,128]{1,0:T(8,128)(2,1)}, u32[]{:S(2)}) copy-start(bf16[128,128]{1,0:T(8,128)(2,1)} %param.27) | copy-start | bytes 98308
  (22 other events, 68.2 us)
Sparse Core Ops, SparseCore 0:
  41.7 48.2 all-gather.5
  231.3 44.5 all-gather.7
where the time goes:
time: 290 us
  waiting for transfers between devices  100 us (34%)
  blocking collectives  98.5 us (34%)
  starting transfers between devices  24.5 us (8%)
  local copies, waits for them, and re-layouts  19.1 us (7%)
  matrix products  17.8 us (6%)
  between operations  14.7 us (5%)
  other arithmetic  14.5 us (5%)
    all_gather x3, blocking collectives, prefix_by_axis(): pieces = jax.tree.map(lambda part: lax.all_gather(part, axis), running)  57.2 us
    all_to_all x1, waiting for transfers between devices, body(): lax.all_to_all(pieces, 'tp', split_axis=1, concat_axis=1, tiled=True)  49 us
    all_gather x1, waiting for transfers between devices, in_one_piece(): out = lax.all_gather(both, axis, axis=dim, tiled=True)  48.4 us
    all_to_all x1, blocking collectives, sent_together(): lax.all_to_all(both, axis, split_axis=split_dim, concat_axis=concat_dim,...  24.5 us
    all_gather x1, blocking collectives, body(): whole = lax.all_gather(d_input, 'tp', axis=1, tiled=True)  16.8 us
    all_to_all x1, starting transfers between devices, body(): lax.all_to_all(summed, SP, split_axis=0, concat_axis=0, tiled=True)  10.5 us
    all_to_all x1, starting transfers between devices, sent_and_summed(): parts = lax.all_to_all(split_up(value, dim, count), axis, 0, 0, tiled=True)  9.32 us
    dot_general x4, matrix products, contract_rows(): lax.dot_general(first_op, second_op, (((0,), (0,)), ((), ())), preferred_...  7.21 us
  transfers between devices with their start and end apart: 5, of which 4 were waited for; matrix products, arithmetic and copies ran while one was open for 8% of the time, Pallas kernels for 0%

commit v1 on v0

--- a/solution.py
+++ b/solution.py
@@ -188,7 +188,8 @@
     d_input = (cot_slice.astype(jnp.float32) + jnp.sum(picked.astype(jnp.float32), axis=1)).astype(
         jnp.bfloat16
     )
-    whole = lax.all_gather(d_input, "tp", axis=1, tiled=True)
+    copies = jnp.concatenate([d_input] * lax.axis_size("tp"), axis=1)
+    whole = lax.all_to_all(copies, "tp", 1, 1, tiled=True)
     back_proj = contract_cols(whole, out_weight)
     pre_act = gate_pre.astype(jnp.float32)
     gate_act = jax.nn.silu(pre_act)

time: 290 us -> 306 us (1.055)
  the two profiles are of different devices: /device:TPU:2 before, /device:TPU:4 now
where the time goes in v1:
time: 306 us; the launch traced here: 305 us
  blocking collectives  138 us (45%)
  waiting for transfers between devices  65.8 us (22%)
  local copies, waits for them, and re-layouts  32.7 us (11%)
  starting transfers between devices  21.3 us (7%)
  matrix products  17.9 us (6%)
  other arithmetic  15.1 us (5%)
  between operations  14.7 us (5%)
    all_gather x3, blocking collectives, prefix_by_axis(): pieces = jax.tree.map(lambda part: lax.all_gather(part, axis), running)  59.2 us
    all_to_all x1, blocking collectives, body(): lax.all_to_all(pieces, 'tp', split_axis=1, concat_axis=1, tiled=True)  53.9 us
    all_gather x1, waiting for transfers between devices, in_one_piece(): out = lax.all_gather(both, axis, axis=dim, tiled=True)  48.5 us
    all_to_all x1, blocking collectives, sent_together(): lax.all_to_all(both, axis, split_axis=split_dim, concat_axis=concat_dim,...  24.4 us
    unnamed x98, local copies, waits for them, and re-layouts  14 us
    all_to_all x1, starting transfers between devices, body(): lax.all_to_all(summed, SP, split_axis=0, concat_axis=0, tiled=True)  10.5 us
    all_to_all x1, waiting for transfers between devices, body(): lax.all_to_all(summed, SP, split_axis=0, concat_axis=0, tiled=True)  9.24 us
    dot_general x4, matrix products, contract_rows(): lax.dot_general(first_op, second_op, (((0,), (0,)), ((), ())), preferred_...  7.41 us
  transfers between devices with their start and end apart: 5, of which 4 were waited for; matrix products, arithmetic and copies ran while one was open for 7% of the time, Pallas kernels for 0%

profile of v1, /device:TPU:4, one launch (start us, length us, event | category | flops | bytes accessed | tf_op | source)
XLA Modules:
  0.0 305.2 jit_solution(14104793886351455867)
XLA Ops:
  11.2 1.4 scatter_custom_fusion
  16.4 24.4 %all_to_all.32 = bf16[32,32,128]{2,1,0:T(8,128)(2,1)S(1)} all-to-all(bf16[32,32,128]{2,1,0:T(8,128)(2,1)S(1)} %pad_maximum_fusion), channel_id=1, replica_groups=mesh['sp_0'=8,'sp_1'=4,'tp'=16] {'sp_0','sp_1'}, dimensions={0} | all-to-all | bytes 524288 | tf_op jit(solution)/shard_map/all_to_all | solution.py:19
  41.6 48.5 %all-gather.6.cloned.1.call-done = bf16[64,16,2048]{2,1,0:T(8,128)(2,1)} async-done(((bf16[64,16,128]{2,1,0:T(8,128)(2,1)}), bf16[64,16,2048]{2,1,0:T(8,128)(2,1)}) %all-gather.6.cloned.1.call-update) | async-done | bytes 4194320 | tf_op jit(solution)/shard_map/all_gather | solution.py:26
  90.0 2.8 fusion.78
  97.6 53.9 %all_to_all.33 = bf16[512,16,128]{2,0,1:T(8,128)(2,1)} all-to-all(bf16[512,16,128]{2,0,1:T(8,128)(2,1)S(1)} %bitcast.238), channel_id=1, replica_groups=mesh['sp_0'=8,'sp_1'=4,'tp'=16] {'tp'}, dimensions={1} | all-to-all | bytes 4194304 | tf_op jit(solution)/shard_map/all_to_all | solution.py:179
  151.5 2.6 reduce_sum.56
  154.1 10.5 %all-to-all-start.2 = ((bf16[32,16,128]{2,1,0:T(8,128)(2,1)}), bf16[32,16,128]{2,1,0:T(8,128)(2,1)S(1)}, u32[]{:S(2)}, u32[]{:S(2)}) async-start(bf16[32,16,128]{2,1,0:T(8,128)(2,1)} %bitcast.14), calls=%async_computation.2 | async-start | bytes 262144 | tf_op jit(solution)/shard_map/all_to_all | solution.py:185
  164.6 9.2 %all-to-all-done.2 = bf16[32,16,128]{2,1,0:T(8,128)(2,1)S(1)} async-done(((bf16[32,16,128]{2,1,0:T(8,128)(2,1)}), bf16[32,16,128]{2,1,0:T(8,128)(2,1)S(1)}, u32[]{:S(2)}, u32[]{:S(2)}) %all-to-all-start.2) | async-done | bytes 131104 | tf_op jit(solution)/shard_map/all_to_all | solution.py:185
  174.9 1.4 constant_dynamic-update-slice_fusion.15
  185.6 2.1 copy.88
  187.7 2.0 copy.89
  189.8 4.2 %all-to-all-start.3 = ((bf16[128,16,128]{2,0,1:T(8,128)(2,1)}), bf16[128,16,128]{2,0,1:T(8,128)(2,1)}, u32[]{:S(2)}, u32[]{:S(2)}) async-start(bf16[128,16,128]{2,0,1:T(8,128)(2,1)} %copy.89), calls=%async_computation.3 | async-start | bytes 1048576 | tf_op jit(solution)/shard_map/all_to_all | solution.py:192
  194.3 7.7 %all-gather.1 = f32[4,1,4]{2,1,0:T(1,128)S(1)} all-gather(f32[1,1,4]{2,1,0:T(1,128)S(1)} %get-tuple-element.67), channel_id=1, replica_groups=mesh['sp_0'=8,'sp_1'=4,'tp'=16] {'sp_1'}, dimensions={0}, use_global_device_ids=true | all-gather | bytes 80 | tf_op jit(solution)/shard_map/all_gather | solution.py:52
  202.6 7.3 %all-to-all-done.3 = bf16[128,16,128]{2,0,1:T(8,128)(2,1)} async-done(((bf16[128,16,128]{2,0,1:T(8,128)(2,1)}), bf16[128,16,128]{2,0,1:T(8,128)(2,1)}, u32[]{:S(2)}, u32[]{:S(2)}) %all-to-all-start.3) | async-done | bytes 524320 | tf_op jit(solution)/shard_map/all_to_all | solution.py:192
  209.9 2.1 copy.90
  212.0 2.9 fusion.57
  214.9 6.5 %all-to-all-start.4 = ((f32[32,64,256]{2,1,0:T(8,128)}), f32[32,64,256]{2,1,0:T(8,128)}, u32[]{:S(2)}, u32[]{:S(2)}) async-start(f32[32,64,256]{2,1,0:T(8,128)} %fusion.57), calls=%async_computation.4 | async-start | bytes 4194304 | tf_op jit(solution)/shard_map/all_to_all | solution.py:37
  222.6 2.2 fusion.21
  226.0 19.2 %all-gather = f32[16,64,128]{2,1,0:T(8,128)S(1)} all-gather(f32[4,64,128]{2,1,0:T(8,128)S(1)} %fusion.54), channel_id=2, replica_groups=mesh['sp_0'=8,'sp_1'=4,'tp'=16] {'sp_1'}, dimensions={0}, use_global_device_ids=true | all-gather | bytes 655360 | tf_op jit(solution)/shard_map/all_gather | solution.py:52
  249.0 1.6 copy.97
  250.6 32.3 %all-gather.2 = f32[8,1,4]{2,1,0:T(1,128)S(1)} all-gather(f32[1,1,4]{2,1,0:T(1,128)} %get-tuple-element.78), channel_id=1, replica_groups=mesh['sp_0'=8,'sp_1'=4,'tp'=16] {'sp_0'}, dimensions={0}, use_global_device_ids=true | all-gather | bytes 144 | tf_op jit(solution)/shard_map/all_gather | solution.py:52
  284.3 2.2 fusion.1
  291.6 1.6 fusion.37
  296.0 2.3 reduce_sum.58
  (163 shorter events, 39.6 us)
Async XLA Ops:
  7.2 215.4 %copy-start = (bf16[256,2048]{1,0:T(8,128)(2,1)S(1)}, bf16[256,2048]{1,0:T(8,128)(2,1)}, u32[]{:S(2)}) copy-start(bf16[256,2048]{1,0:T(8,128)(2,1)} %param.22) | copy-start | bytes 3145732
  7.2 82.9 %all-gather.6.cloned.1.call-start = ((), (), s32[]{:S(2)}) async-start(), calls=%async_computation.5 | async-start | bytes 4456448 | tf_op jit(solution)/shard_map/all_gather | solution.py:26
  41.6 51.3 %copy-start.6 = (bf16[1,2048,64]{1,2,0:T(8,128)(2,1)S(1)}, bf16[1,2048,64]{1,2,0:T(8,128)(2,1)}, u32[]{:S(2)}) copy-start(bf16[1,2048,64]{1,2,0:T(8,128)(2,1)} %param.19) | copy-start | bytes 786436
  154.1 19.8 %all-to-all-start.2 = ((bf16[32,16,128]{2,1,0:T(8,128)(2,1)}), bf16[32,16,128]{2,1,0:T(8,128)(2,1)S(1)}, u32[]{:S(2)}, u32[]{:S(2)}) async-start(bf16[32,16,128]{2,1,0:T(8,128)(2,1)} %bitcast.14), calls=%async_computation.2 | async-start | bytes 262144 | tf_op jit(solution)/shard_map/all_to_all | solution.py:185
  176.3 17.9 %copy-start.1 = (bf16[128,128]{1,0:T(8,128)(2,1)}, bf16[128,128]{1,0:T(8,128)(2,1)S(1)}, u32[]{:S(2)}) copy-start(bf16[128,128]{1,0:T(8,128)(2,1)S(1)} %get-tuple-element.55) | copy-start | bytes 98308
  176.3 17.7 %copy-start.36 = (f32[4,128]{1,0:T(4,128)S(1)}, f32[4,128]{1,0:T(4,128)}, u32[]{:S(2)}) copy-start(f32[4,128]{1,0:T(4,128)} %param.28) | copy-start | bytes 6148
  185.6 26.4 %copy-start.20 = (bf16[128,256]{1,0:T(8,128)(2,1)S(1)}, bf16[128,256]{1,0:T(8,128)(2,1)}, u32[]{:S(2)}) copy-start(bf16[128,256]{1,0:T(8,128)(2,1)} %param.24) | copy-start | bytes 196612
  189.8 20.2 %all-to-all-start.3 = ((bf16[128,16,128]{2,0,1:T(8,128)(2,1)}), bf16[128,16,128]{2,0,1:T(8,128)(2,1)}, u32[]{:S(2)}, u32[]{:S(2)}) async-start(bf16[128,16,128]{2,0,1:T(8,128)(2,1)} %copy.89), calls=%async_computation.3 | async-start | bytes 1048576 | tf_op jit(solution)/shard_map/all_to_all | solution.py:192
  214.9 81.1 %all-to-all-start.4 = ((f32[32,64,256]{2,1,0:T(8,128)}), f32[32,64,256]{2,1,0:T(8,128)}, u32[]{:S(2)}, u32[]{:S(2)}) async-start(f32[32,64,256]{2,1,0:T(8,128)} %fusion.57), calls=%async_computation.4 | async-start | bytes 4194304 | tf_op jit(solution)/shard_map/all_to_all | solution.py:37
  221.4 4.4 %copy-start.12 = (bf16[128,128]{1,0:T(8,128)(2,1)S(1)}, bf16[128,128]{1,0:T(8,128)(2,1)}, u32[]{:S(2)}) copy-start(bf16[128,128]{1,0:T(8,128)(2,1)} %param.27) | copy-start | bytes 98308
  221.4 70.1 %all-gather.8.cloned.1.call-start = ((), (), s32[]{:S(2)}) async-start(), calls=%async_computation.6 | async-start | bytes 1179648 | tf_op jit(solution)/shard_map/all_gather | solution.py:52
  222.0 25.5 %copy-start.24 = (f32[4]{0:T(128)}, f32[4]{0:T(128)S(1)}, u32[]{:S(2)}) copy-start(f32[4]{0:T(128)S(1)} %get-tuple-element.80) | copy-start | bytes 52
  222.6 61.0 %copy-start.10 = (bf16[128,128]{1,0:T(8,128)(2,1)S(1)}, bf16[128,128]{1,0:T(8,128)(2,1)}, u32[]{:S(2)}) copy-start(bf16[128,128]{1,0:T(8,128)(2,1)} %param.26) | copy-start | bytes 98308
  250.6 35.9 %copy-start.15 = (bf16[512,64]{0,1:T(8,128)(2,1)S(1)}, bf16[512,64]{0,1:T(8,128)(2,1)}, u32[]{:S(2)}) copy-start(bf16[512,64]{0,1:T(8,128)(2,1)} %copy-done.14) | copy-start | bytes 196612
  282.9 6.5 %copy-start.22 = (pred[128,128]{1,0:T(8,128)(4,1)}, pred[128,128]{1,0:T(8,128)(4,1)S(1)}, u32[]{:S(2)}) copy-start(pred[128,128]{1,0:T(8,128)(4,1)S(1)} %iota_compare_fusion) | copy-start | bytes 49156
  287.7 3.8 %copy-start.5 = (f32[16,64,128]{2,1,0:T(8,128)S(1)}, f32[16,64,128]{2,1,0:T(8,128)}, u32[]{:S(2)}) copy-start(f32[16,64,128]{2,1,0:T(8,128)} %copy-done.4) | copy-start | bytes 1572868
  287.7 3.8 %copy-start.25 = (f32[4]{0:T(128)S(1)}, f32[4]{0:T(128)}, u32[]{:S(2)}) copy-start(f32[4]{0:T(128)} %copy-done.24) | copy-start | bytes 52
  287.7 3.8 %copy-start.26 = (f32[4]{0:T(128)S(1)}, f32[4]{0:T(128)}, u32[]{:S(2)}) copy-start(f32[4]{0:T(128)} %get-tuple-element.81) | copy-start | bytes 52
  287.7 3.8 %copy-start.27 = (f32[4]{0:T(128)S(1)}, f32[4]{0:T(128)}, u32[]{:S(2)}) copy-start(f32[4]{0:T(128)} %get-tuple-element.76) | copy-start | bytes 52
  287.8 3.8 %copy-start.28 = (f32[4]{0:T(128)S(1)}, f32[4]{0:T(128)}, u32[]{:S(2)}) copy-start(f32[4]{0:T(128)} %get-tuple-element.68) | copy-start | bytes 52
  289.0 4.4 %copy-start.21 = (f32[128,128]{1,0:T(8,128)S(1)}, f32[128,128]{1,0:T(8,128)}, u32[]{:S(2)}) copy-start(f32[128,128]{1,0:T(8,128)} %fusion.80) | copy-start | bytes 196612
  289.0 4.4 %copy-start.38 = (f32[128,4]{0,1:T(4,128)S(1)}, f32[128,4]{0,1:T(4,128)}, u32[]{:S(2)}) copy-start(f32[128,4]{0,1:T(4,128)} %copy.93) | copy-start | bytes 6148
  289.0 5.7 %copy-start.18 = (bf16[128,256]{0,1:T(8,128)(2,1)S(1)}, bf16[128,256]{0,1:T(8,128)(2,1)}, u32[]{:S(2)}) copy-start(bf16[128,256]{0,1:T(8,128)(2,1)} %copy.97) | copy-start | bytes 196612
  289.0 6.1 %copy-start.13 = (bf16[128,128]{1,0:T(8,128)(2,1)S(1)}, bf16[128,128]{1,0:T(8,128)(2,1)}, u32[]{:S(2)}) copy-start(bf16[128,128]{1,0:T(8,128)(2,1)} %param.27) | copy-start | bytes 98308
  (21 other events, 56.3 us)
Sparse Core Ops, SparseCore 0:
  41.7 48.2 all-gather.5
  247.6 43.9 all-gather.7
